TPU v7x, 32 devices: a whole 2x2x4 slice. The times are simulated.
32 devices in a mesh: sp: 4 (over z), tp: 2 (over y), dp: 4 (over x, core).
Axes of the slice: x: 2, y: 2, z: 4, core: 2. Of those that a mesh axis runs over, the one named last changes fastest.
Arguments:
- latent: bfloat16 [5120, 3072], P(('dp', 'sp', 'tp')), parts along dimension 0, may hold values from -6 to 6
- condition: float32 [12288], P('dp'), parts along dimension 0, may hold values from -8 to 8
- ctx_condition: float32 [3072], replicated, may hold values from -8 to 8
- context: bfloat16 [512, 3072], P(('dp', 'sp')), parts along dimension 0, may hold values from -6 to 6
- mod_shift: bfloat16 [3072, 3072], P('sp', 'tp'), may hold values from -0.109375 to 0.109375
- mod_scale: bfloat16 [3072, 3072], P('sp', 'tp'), may hold values from -0.109375 to 0.109375
- mod_gate: bfloat16 [3072, 3072], P('sp', 'tp'), may hold values from -0.109375 to 0.109375
- norm_gain: float32 [3072], replicated, may hold values from 0.5 to 6
- w_query: bfloat16 [3072, 3072], P(None, 'tp'), may hold values from -0.109375 to 0.109375
- key_weight: bfloat16 [3072, 512], P(None, 'tp'), may hold values from -0.109375 to 0.109375
- value_weight: bfloat16 [3072, 512], P(None, 'tp'), may hold values from -0.109375 to 0.109375
- w_gate: bfloat16 [3072, 3072], P(None, 'tp'), may hold values from -0.109375 to 0.109375
- w_out: bfloat16 [3072, 3072], P('tp'), may hold values from -1.5 to 1.5
- sink_logit: float32 [48], P('tp'), may hold values from 4 to 7.5
Outputs:
- updated_latent: bfloat16 [5120, 3072], P(('dp', 'sp', 'tp')), parts along dimension 0
There are 4 independent parts, one for each index of `dp`. A program takes and returns all parts, laid end to end along the dimension named above; an argument that names none is the same for every part. Nothing has to cross between parts.
All inputs are finite; a program needn't handle non-finite values.
Results may differ from a plain program's by a relative error of at most 0.02.
The roundings to bfloat16 on the way count: a program that leaves them out, or rounds other values in their place, can miss the bound.
Values may be sent and summed in bfloat16 or wider, within the bound.
A program may use at most 128 MiB of HBM per device.

v0:
```python
import math

import jax
import jax.numpy as jnp
from jax import lax
from jax.sharding import PartitionSpec as P

HEAD_SIZE = 64
WINDOW = 128
GRID_W = 64


NORM_EPS = 1e-06
MASK_VALUE = -1e30


def with_halo(block, sides, width):
    for axis, dim in sides:
        count = lax.axis_size(axis)
        forward = [(i, i + 1) for i in range(count - 1)]
        backward = [(target, source) for source, target in forward]
        low = lax.ppermute(
            lax.slice_in_dim(block, block.shape[dim] - width, None, axis=dim), axis, forward
        )
        high = lax.ppermute(lax.slice_in_dim(block, 0, width, axis=dim), axis, backward)
        block = jnp.concatenate([low, block, high], axis=dim)
    return block


def modulate(row_data, gain_vec, shift_vec, scale_vec):
    values = row_data.astype(jnp.float32)
    inverse = lax.rsqrt(jnp.mean(values * values, axis=-1, keepdims=True) + NORM_EPS)
    return (values * inverse * gain_vec * (1.0 + scale_vec) + shift_vec).astype(jnp.bfloat16)


def rotate(projected, positions):
    row_count = projected.shape[0]
    head_count = projected.shape[1] // HEAD_SIZE
    quarter = HEAD_SIZE // 4
    half_dim = HEAD_SIZE // 2
    inverse = jnp.exp(-math.log(10000.0) * jnp.arange(quarter, dtype=jnp.float32) / quarter)
    grid_row = (positions // GRID_W).astype(jnp.float32)
    mesh_column = (positions % GRID_W).astype(jnp.float32)
    angles = jnp.concatenate([grid_row[:, None] * inverse, mesh_column[:, None] * inverse], axis=1)
    cosine = jnp.cos(angles)[:, None, :]
    sine_table = jnp.sin(angles)[:, None, :]
    shaped = projected.reshape(row_count, head_count, HEAD_SIZE)
    first_half = shaped[..., :half_dim]
    second = shaped[..., half_dim:]
    turned = jnp.concatenate(
        [first_half * cosine - second * sine_table, second * cosine + first_half * sine_table],
        axis=-1,
    )
    return turned.reshape(row_count, head_count * HEAD_SIZE)


def attend(
    queries, key_rows, value_rows, ctx_keys, ctx_values, sink_logit, q_begin, k_begin, seq_total
):
    row_count = queries.shape[0]
    key_count = key_rows.shape[0]
    ctx_count = ctx_keys.shape[0]
    kv_heads = key_rows.shape[1] // HEAD_SIZE
    head_count = queries.shape[1] // HEAD_SIZE
    group_size = head_count // kv_heads
    factor = 1.0 / math.sqrt(HEAD_SIZE)
    q_heads = queries.reshape(row_count, kv_heads, group_size, HEAD_SIZE)
    k_heads = key_rows.reshape(key_count, kv_heads, HEAD_SIZE)
    v_heads = value_rows.reshape(key_count, kv_heads, HEAD_SIZE)
    ck_heads = ctx_keys.reshape(ctx_count, kv_heads, HEAD_SIZE)
    cv_heads = ctx_values.reshape(ctx_count, kv_heads, HEAD_SIZE)
    near_scores = (
        jnp.einsum("qkgd,skd->kgqs", q_heads, k_heads, preferred_element_type=jnp.float32) * factor
    )
    q_pos = q_begin + jnp.arange(row_count, dtype=jnp.int32)
    k_pos = k_begin + jnp.arange(key_count, dtype=jnp.int32)
    in_window = (jnp.abs(q_pos[:, None] - k_pos[None, :]) <= WINDOW) & (
        (k_pos >= 0) & (k_pos < seq_total)
    )[None, :]
    near_scores = jnp.where(in_window, near_scores, MASK_VALUE)
    ctx_scores = (
        jnp.einsum("qkgd,skd->kgqs", q_heads, ck_heads, preferred_element_type=jnp.float32) * factor
    )
    sink_score = sink_logit.reshape(kv_heads, group_size)[:, :, None, None]
    peak_score = jnp.maximum(
        jnp.maximum(
            jnp.max(near_scores, axis=-1, keepdims=True),
            jnp.max(ctx_scores, axis=-1, keepdims=True),
        ),
        sink_score,
    )
    near_exp = jnp.exp(near_scores - peak_score)
    ctx_exp = jnp.exp(ctx_scores - peak_score)
    softmax_denominator = (
        jnp.sum(near_exp, axis=-1, keepdims=True)
        + jnp.sum(ctx_exp, axis=-1, keepdims=True)
        + jnp.exp(sink_score - peak_score)
    )
    near_weights = (near_exp / softmax_denominator).astype(jnp.bfloat16)
    ctx_weights = (ctx_exp / softmax_denominator).astype(jnp.bfloat16)
    result = jnp.einsum("kgqs,skd->qkgd", near_weights, v_heads, preferred_element_type=jnp.float32)
    result = result + jnp.einsum(
        "kgqs,skd->qkgd", ctx_weights, cv_heads, preferred_element_type=jnp.float32
    )
    return result.reshape(row_count, head_count * HEAD_SIZE)


def shards(
    latent,
    condition,
    ctx_condition,
    context,
    mod_shift,
    mod_scale,
    mod_gate,
    norm_gain,
    w_query,
    key_weight,
    value_weight,
    w_gate,
    w_out,
    sink_logit,
):
    sp_count = lax.axis_size("sp")
    sp_rank = lax.axis_index("sp")
    mod_rows = mod_shift.shape[0]
    cond_act = jax.nn.silu(condition).astype(jnp.bfloat16)
    ctx_act = jax.nn.silu(ctx_condition).astype(jnp.bfloat16)
    first_row = sp_rank * mod_rows
    lat_piece = lax.dynamic_slice_in_dim(cond_act, first_row, mod_rows, 0)
    ctx_piece = lax.dynamic_slice_in_dim(ctx_act, first_row, mod_rows, 0)
    both_conds = jnp.stack([lat_piece, ctx_piece])
    partial_value = jnp.concatenate(
        [
            jnp.dot(both_conds, mod_shift, preferred_element_type=jnp.float32),
            jnp.dot(both_conds, mod_scale, preferred_element_type=jnp.float32),
            jnp.dot(lat_piece[None, :], mod_gate, preferred_element_type=jnp.float32),
        ],
        axis=0,
    )
    summed = lax.psum(partial_value, "sp")
    vectors = lax.all_gather(summed, "tp", axis=1, tiled=True)
    lat_shift = vectors[0]
    ctx_shift = vectors[1]
    lat_scale = vectors[2]
    ctx_scale = vectors[3]
    lat_gate = vectors[4]
    hidden = modulate(latent, norm_gain, lat_shift, lat_scale)
    ctx_hidden = modulate(context, norm_gain, ctx_shift, ctx_scale)
    kv_width = key_weight.shape[1]
    q_width = w_query.shape[1]
    ctx_pair = jnp.concatenate(
        [
            jnp.dot(ctx_hidden, key_weight, preferred_element_type=jnp.float32).astype(
                jnp.bfloat16
            ),
            jnp.dot(ctx_hidden, value_weight, preferred_element_type=jnp.float32).astype(
                jnp.bfloat16
            ),
        ],
        axis=1,
    )
    ctx_all = lax.all_gather(ctx_pair, "sp", axis=0, tiled=True)
    row_piece = lax.all_gather(hidden, "tp", axis=0, tiled=True)
    projected = jnp.concatenate(
        [
            jnp.dot(row_piece, w_query, preferred_element_type=jnp.float32),
            jnp.dot(row_piece, key_weight, preferred_element_type=jnp.float32),
            jnp.dot(row_piece, value_weight, preferred_element_type=jnp.float32),
            jnp.dot(row_piece, w_gate, preferred_element_type=jnp.float32),
        ],
        axis=1,
    )
    block_rows = projected.shape[0]
    q_begin = sp_rank * block_rows
    positions = q_begin + jnp.arange(block_rows, dtype=jnp.int32)
    queries = rotate(projected[:, :q_width], positions).astype(jnp.bfloat16)
    key_rows = rotate(projected[:, q_width : q_width + kv_width], positions).astype(jnp.bfloat16)
    value_rows = projected[:, q_width + kv_width : q_width + 2 * kv_width].astype(jnp.bfloat16)
    gate_proj = projected[:, q_width + 2 * kv_width :].astype(jnp.bfloat16)
    key_value = jnp.concatenate([key_rows, value_rows], axis=1)
    padded = with_halo(key_value, (("sp", 0),), WINDOW)
    attended = attend(
        queries,
        padded[:, :kv_width],
        padded[:, kv_width:],
        ctx_all[:, :kv_width],
        ctx_all[:, kv_width:],
        sink_logit,
        q_begin,
        q_begin - WINDOW,
        block_rows * sp_count,
    )
    mixed = (attended * jax.nn.silu(gate_proj.astype(jnp.float32))).astype(jnp.bfloat16)
    branch = lax.psum_scatter(
        jnp.dot(mixed, w_out, preferred_element_type=jnp.float32).astype(jnp.bfloat16),
        "tp",
        scatter_dimension=0,
        tiled=True,
    ).astype(jnp.float32)
    return (latent.astype(jnp.float32) + lat_gate * branch).astype(jnp.bfloat16)


def solution(mesh):
    return jax.shard_map(
        shards,
        mesh=mesh,
        in_specs=(
            P(("dp", "sp", "tp"), None),
            P("dp"),
            P(),
            P(("dp", "sp"), None),
            P("sp", "tp"),
            P("sp", "tp"),
            P("sp", "tp"),
            P(),
            P(None, "tp"),
            P(None, "tp"),
            P(None, "tp"),
            P(None, "tp"),
            P("tp", None),
            P("tp"),
        ),
        out_specs=P(("dp", "sp", "tp"), None),
        check_vma=False,
    )
```

profile of v0, /device:TPU:0, one launch (start us, length us, event | category | flops | bytes accessed | tf_op | source)
XLA Modules:
  0.0 179.3 jit_solution(17299851433781400490)
XLA Ops:
  6.5 0.9 multiply_convert_fusion.1
  10.5 21.4 %psum.7 = f32[5,1536]{1,0:T(8,128)S(1)} all-reduce(f32[5,1536]{1,0:T(8,128)S(1)} %pad_maximum_fusion.5), channel_id=1, replica_groups=mesh['sp'=4,'tp'=2,'dp'=4] {'sp'}, use_global_device_ids=true, to_apply=%region_0.1 | all-reduce | flops 7680 | bytes 61440 | tf_op jit(solution)/shard_map/psum | solution.py:141
  31.9 4.8 %all_gather.9 = f32[5,3072]{1,0:T(8,128)S(1)} all-gather(f32[5,1536]{1,0:T(8,128)S(1)} %psum.7), channel_id=1, replica_groups=mesh['sp'=4,'tp'=2,'dp'=4] {'tp'}, dimensions={1}, use_global_device_ids=true | all-gather | bytes 92160 | tf_op jit(solution)/shard_map/all_gather | solution.py:142
  37.0 1.4 fusion.10
  39.1 1.8 %convolution_convert_fusion.3 = bf16[32,256]{1,0:T(8,128)(2,1)S(1)} fusion(bf16[3072,256]{1,0:T(8,128)(2,1)} %param.24, bf16[32,3072]{1,0:T(8,128)(2,1)S(1)} %copy-done.7, f32[3072]{0:T(1024)S(1)} %bitcast.93, f32[3072]{0:T(1024)S(1)} %bitcast.95, f32[3072]{0:T(1024)S(1)} %copy-done.9, f32[32]{0:T(128)S(1)} %add_rsqrt_fusion.1), kind=kOutput, calls=%fused_computation.30 | convolution fusion | flops 50929664 | bytes 1822848 | tf_op jit(solution)/shard_map/dot_general | solution.py:157
  41.0 13.4 %all_gather.11 = bf16[128,512]{1,0:T(8,128)(2,1)S(1)} all-gather(bf16[32,512]{1,0:T(8,128)(2,1)S(1)} %pad_maximum_fusion.7), channel_id=1, replica_groups=mesh['sp'=4,'tp'=2,'dp'=4] {'sp'}, dimensions={0}, use_global_device_ids=true | all-gather | bytes 163840 | tf_op jit(solution)/shard_map/all_gather | solution.py:163
  55.3 13.1 %all-gather.2.cloned.1.call-done = bf16[320,3072]{1,0:T(8,128)(2,1)} async-done(((bf16[160,3072]{1,0:T(8,128)(2,1)}), bf16[320,3072]{1,0:T(8,128)(2,1)}) %all-gather.2.cloned.1.call-update) | async-done | bytes 1966096 | tf_op jit(solution)/shard_map/all_gather | solution.py:164
  68.4 2.6 %fusion.38 = f32[320,256]{0,1:T(8,128)S(1)} fusion(bf16[320,3072]{1,0:T(8,128)(2,1)} %all-gather.2.cloned.1.call-done, bf16[3072,256]{1,0:T(8,128)(2,1)S(1)} %copy-done.8), kind=kOutput, calls=%fused_computation.87 | convolution fusion | flops 503316480 | bytes 3866624 | tf_op jit(solution)/shard_map/dot_general | solution.py:168
  71.3 2.8 %convolution_convert_fusion.2 = bf16[320,256]{1,0:T(8,128)(2,1)S(1)} fusion(bf16[320,3072]{1,0:T(8,128)(2,1)} %all-gather.2.cloned.1.call-done, bf16[3072,256]{1,0:T(8,128)(2,1)} %param.24), kind=kOutput, calls=%fused_computation.29 | convolution fusion | flops 503398400 | bytes 3702784 | tf_op jit(solution)/shard_map/dot_general | solution.py:169
  74.1 3.4 %collective-permute-start = (bf16[128,512]{1,0:T(8,128)(2,1)S(1)}, bf16[128,512]{1,0:T(8,128)(2,1)S(1)}, u32[]{:S(2)}, u32[]{:S(2)}) collective-permute-start(bf16[128,512]{1,0:T(8,128)(2,1)S(1)} %get-tuple-element.11), channel_id=1, source_target_pairs={{0,8},{8,16},{16,24},{1,9},{9,17},{17,25},{2,10},{10,18},{18,26},{... | collective-permute-start | bytes 393224 | tf_op jit(solution)/shard_map/ppermute | solution.py:22
  77.5 1.5 collective-permute-start.1
  79.0 7.7 %fusion.39 = f32[320,1536]{0,1:T(8,128)S(1)} fusion(bf16[320,3072]{1,0:T(8,128)(2,1)S(1)} %copy-done.11, bf16[3072,1536]{1,0:T(8,128)(2,1)} %param.22), kind=kOutput, calls=%fused_computation.88 | convolution fusion | flops 3019898880 | bytes 13369344 | tf_op jit(solution)/shard_map/dot_general | solution.py:167
  87.3 2.8 %bitcast_reduce_fusion = (f32[4,6,320]{2,1,0:T(8,128)S(1)}, f32[4,128,320,6]{1,2,3,0:T(8,128)}) fusion(bf16[128,4,64,1]{0,2,3,1:T(8,128)(2,1)S(1)} %bitcast.91, bf16[320,4,6,64]{0,3,2,1:T(8,128)(2,1)S(1)} %bitcast.83), kind=kOutput, calls=%fused_computation.8 | convolution fusion | flops 127787520 | bytes 5011456 | tf_op jit(solution)/shard_map/qkgd,skd->kgqs/dot_general | solution.py:82
  90.1 0.8 fusion.34
  90.9 1.2 copy.24
  92.1 4.5 %fusion.1 = (f32[4,6,320]{2,1,0:T(8,128)S(1)}, f32[4,576,320,6]{1,2,3,0:T(8,128)S(1)}) fusion(pred[320,576]{1,0:T(8,128)(4,1)S(1)} %fusion.14, bf16[576,4,64,1]{0,2,3,1:T(8,128)(2,1)S(1)} %bitcast.87, bf16[320,4,6,64]{0,3,2,1:T(8,128)(2,1)S(1)} %bitcast.84), kind=kOutput, calls=%fused_computation.4 | convolution fusion | flops 579494400 | bytes 19187712 | tf_op jit(solution)/shard_map/qkgd,skd->kgqs/dot_general | solution.py:73
  96.7 2.6 %fusion.4 = f32[4,6,320]{2,1,0:T(8,128)S(1)} fusion(f32[4,128,320,6]{1,2,3,0:T(8,128)S(1)} %copy-done.3, f32[4,6,320]{2,1,0:T(8,128)S(1)} %maximum_maximum_fusion), kind=kLoop, calls=%fused_computation.11 | loop fusion | flops 2941440 | bytes 3993600 | tf_op jit(solution)/shard_map/reduce_sum | solution.py:96
  99.3 5.5 %fusion = f32[4,6,320]{2,1,0:T(8,128)S(1)} fusion(f32[4,576,320,6]{1,2,3,0:T(8,128)S(1)} %get-tuple-element.25, f32[4,6,320]{2,1,0:T(8,128)S(1)} %maximum_maximum_fusion, pred[320,576]{1,0:T(8,128)(4,1)S(1)} %fusion.14), kind=kLoop, calls=%fused_computation.3 | loop fusion | flops 17687040 | bytes 17940480 | tf_op jit(solution)/shard_map/reduce_sum | solution.py:95
  105.0 5.7 %fusion.12 = f32[4,64,6,320]{3,1,2,0:T(8,128)S(1)} fusion(bf16[128,4,64,1]{0,2,3,1:T(8,128)(2,1)S(1)} %bitcast.96, f32[4,128,320,6]{1,2,3,0:T(8,128)} %get-tuple-element.27, f32[4,6,320]{2,1,0:T(8,128)S(1)} %exponential_add_fusion, f32[4,6,320]{2,1,0:T(8,128)S(1)} %maximum_maximum_fusion), kind=kOutput, calls=%fused_computation.24 | convolution fusion | flops 129761280 | bytes 6025216 | tf_op jit(solution)/shard_map/kgqs,skd->qkgd/dot_general | solution.py:102
  110.7 10.9 %fusion.13 = f32[4,64,6,320]{3,1,2,0:T(8,128)} fusion(f32[4,64,6,320]{3,1,2,0:T(8,128)S(1)} %fusion.12, bf16[576,4,64,1]{0,2,3,1:T(8,128)(2,1)S(1)} %bitcast.90, f32[4,576,320,6]{1,2,3,0:T(8,128)} %copy-done.2, f32[4,6,320]{2,1,0:T(8,128)S(1)} %exponential_add_fusion, f32[4,6,320]{2,1,0:T(8,128)S(1)} %maximum_maximum_fusion, pred[320,576]{1,0:T(8,128)(4,1)S(1)} %fusion.14), kind=kOutput, calls=%fused_computation.25 | convolution fusion | flops 588840960 | bytes 22167552 | tf_op jit(solution)/shard_map/kgqs,skd->qkgd/dot_general | solution.py:101
  121.6 2.0 %copy.28 = f32[320,1536]{1,0:T(8,128)S(1)} copy(f32[320,1536]{0,1:T(8,128)} %bitcast.85) | data formatting | bytes 3932160 | tf_op jit(solution)/shard_map/reshape | solution.py:105
  123.6 14.5 %convolution_convert_fusion = bf16[320,3072]{1,0:T(8,128)(2,1)} fusion(bf16[1536,3072]{1,0:T(8,128)(2,1)} %param.26, f32[320,1536]{1,0:T(8,128)S(1)} %copy.28, bf16[320,3072]{1,0:T(8,128)(2,1)} %all-gather.2.cloned.1.call-done, bf16[3072,1536]{1,0:T(8,128)(2,1)} %param.25), kind=kOutput, calls=%fused_computation.6 | convolution fusion | flops 6044712960 | bytes 24772608 | tf_op jit(solution)/shard_map/dot_general | solution.py:196
  138.2 31.8 %reduce-scatter.2.cloned.1.call-done = bf16[160,3072]{1,0:T(8,128)(2,1)} async-done(((bf16[320,3072]{1,0:T(8,128)(2,1)}), bf16[160,3072]{1,0:T(8,128)(2,1)}) %reduce-scatter.2.cloned.1.call-update) | async-done | bytes 983056 | tf_op jit(solution)/shard_map/reduce_scatter | solution.py:195
  170.0 2.5 %fusion.11 = bf16[160,3072]{1,0:T(8,128)(2,1)} fusion(bf16[160,3072]{1,0:T(8,128)(2,1)S(1)} %copy-done.4, bf16[160,3072]{1,0:T(8,128)(2,1)} %reduce-scatter.2.cloned.1.call-done, f32[3072]{0:T(1024)S(1)} %bitcast.97), kind=kLoop, calls=%fused_computation.22 | loop fusion | flops 2457600 | bytes 2961408 | tf_op jit(solution)/shard_map/convert_element_type | solution.py:201
  (66 shorter events, 6.1 us)
Async XLA Ops:
  6.5 1.7 copy-start
  6.5 61.9 %all-gather.2.cloned.1.call-start = ((), (), s32[]{:S(2)}) async-start(), calls=%async_computation.1 | async-start | bytes 2949120 | tf_op jit(solution)/shard_map/all_gather | solution.py:164
  6.5 2.4 %copy-start.5 = (bf16[768,1536]{1,0:T(8,128)(2,1)S(1)}, bf16[768,1536]{1,0:T(8,128)(2,1)}, u32[]{:S(2)}) copy-start(bf16[768,1536]{1,0:T(8,128)(2,1)} %param.18) | copy-start | bytes 7077892
  8.2 1.8 %copy-start.6 = (bf16[768,1536]{1,0:T(8,128)(2,1)S(1)}, bf16[768,1536]{1,0:T(8,128)(2,1)}, u32[]{:S(2)}) copy-start(bf16[768,1536]{1,0:T(8,128)(2,1)} %param.20) | copy-start | bytes 7077892
  8.9 27.8 %copy-start.4 = (bf16[160,3072]{1,0:T(8,128)(2,1)S(1)}, bf16[160,3072]{1,0:T(8,128)(2,1)}, u32[]{:S(2)}) copy-start(bf16[160,3072]{1,0:T(8,128)(2,1)} %param.14) | copy-start | bytes 2949124
  10.1 27.0 %copy-start.9 = (f32[3072]{0:T(1024)S(1)}, f32[3072]{0:T(1024)}, u32[]{:S(2)}) copy-start(f32[3072]{0:T(1024)} %param.21) | copy-start | bytes 36868
  10.5 28.0 %copy-start.7 = (bf16[32,3072]{1,0:T(8,128)(2,1)S(1)}, bf16[32,3072]{1,0:T(8,128)(2,1)}, u32[]{:S(2)}) copy-start(bf16[32,3072]{1,0:T(8,128)(2,1)} %param.17) | copy-start | bytes 589828
  10.5 28.2 %copy-start.8 = (bf16[3072,256]{1,0:T(8,128)(2,1)S(1)}, bf16[3072,256]{1,0:T(8,128)(2,1)}, u32[]{:S(2)}) copy-start(bf16[3072,256]{1,0:T(8,128)(2,1)} %param.23) | copy-start | bytes 4718596
  38.4 16.0 %copy-start.10 = (f32[24]{0:T(128)S(1)}, f32[24]{0:T(128)}, u32[]{:S(2)}) copy-start(f32[24]{0:T(128)} %param.27) | copy-start | bytes 292
  38.4 131.5 %reduce-scatter.2.cloned.1.call-start = ((), (), s32[]{:S(2)}) async-start(), calls=%async_computation.2 | async-start | bytes 2949120 | tf_op jit(solution)/shard_map/reduce_scatter | solution.py:195
  71.3 7.7 %copy-start.11 = (bf16[320,3072]{1,0:T(8,128)(2,1)S(1)}, bf16[320,3072]{1,0:T(8,128)(2,1)}, u32[]{:S(2)}) copy-start(bf16[320,3072]{1,0:T(8,128)(2,1)} %all-gather.2.cloned.1.call-done) | copy-start | bytes 5898244
  74.1 16.0 %collective-permute-start = (bf16[128,512]{1,0:T(8,128)(2,1)S(1)}, bf16[128,512]{1,0:T(8,128)(2,1)S(1)}, u32[]{:S(2)}, u32[]{:S(2)}) collective-permute-start(bf16[128,512]{1,0:T(8,128)(2,1)S(1)} %get-tuple-element.11), channel_id=1, source_target_pairs={{0,8},{8,16},{16,24},{1,9},{9,17},{17,25},{2,10},{10,18},{18,26},{... | collective-permute-start | bytes 393224 | tf_op jit(solution)/shard_map/ppermute | solution.py:22
  77.5 12.6 %collective-permute-start.1 = (bf16[128,512]{1,0:T(8,128)(2,1)S(1)}, bf16[128,512]{1,0:T(8,128)(2,1)S(1)}, u32[]{:S(2)}, u32[]{:S(2)}) collective-permute-start(bf16[128,512]{1,0:T(8,128)(2,1)S(1)} %get-tuple-element.12), channel_id=1, source_target_pairs={{8,0},{16,8},{24,16},{9,1},{17,9},{25,17},{10,2},{18,10},{26,18},{... | collective-permute-start | bytes 393224 | tf_op jit(solution)/shard_map/ppermute | solution.py:25
  92.1 4.6 %copy-start.3 = (f32[4,128,320,6]{1,2,3,0:T(8,128)S(1)}, f32[4,128,320,6]{1,2,3,0:T(8,128)}, u32[]{:S(2)}) copy-start(f32[4,128,320,6]{1,2,3,0:T(8,128)} %get-tuple-element.27) | copy-start | bytes 11796484
  96.6 8.1 %copy-start.2 = (f32[4,576,320,6]{1,2,3,0:T(8,128)}, f32[4,576,320,6]{1,2,3,0:T(8,128)S(1)}, u32[]{:S(2)}) copy-start(f32[4,576,320,6]{1,2,3,0:T(8,128)S(1)} %get-tuple-element.25) | copy-start | bytes 53084164
  138.2 34.3 %copy-start.1 = (bf16[768,1536]{1,0:T(8,128)(2,1)S(1)}, bf16[768,1536]{1,0:T(8,128)(2,1)}, u32[]{:S(2)}) copy-start(bf16[768,1536]{1,0:T(8,128)(2,1)} %param.19) | copy-start | bytes 7077892
Sparse Core Ops, SparseCore 0:
  38.6 29.8 all-gather.1
  138.3 31.6 reduce-scatter.1
where the time goes:
time: 180 us; the launch traced here: 179 us
  matrix products  55 us (31%)
  waiting for transfers between devices  44.9 us (25%)
  blocking collectives  39.5 us (22%)
  other arithmetic  14.8 us (8%)
  between operations  13.7 us (8%)
  local copies, waits for them, and re-layouts  6.34 us (4%)
  starting transfers between devices  4.91 us (3%)
    reduce_scatter x1, waiting for transfers between devices, shards(): lax.psum_scatter(jnp.dot(mixed, w_out, preferred_element_type=jnp.float32...  31.8 us
    psum x1, blocking collectives, shards(): summed = lax.psum(partial_value, 'sp')  21.4 us
    dot_general x1, matrix products, shards(): jnp.dot(mixed, w_out, preferred_element_type=jnp.float32)  14.5 us
    all_gather x1, blocking collectives, shards(): ctx_all = lax.all_gather(ctx_pair, 'sp', axis=0, tiled=True)  13.4 us
    all_gather x1, waiting for transfers between devices, shards(): row_piece = lax.all_gather(hidden, 'tp', axis=0, tiled=True)  13.1 us
    dot_general x1, matrix products, attend(): jnp.einsum('kgqs,skd->qkgd', near_weights, v_heads, preferred_element_typ...  10.9 us
    dot_general x1, matrix products, shards(): jnp.dot(row_piece, w_query, preferred_element_type=jnp.float32)  7.75 us
    dot_general x1, matrix products, attend(): jnp.einsum('kgqs,skd->qkgd', ctx_weights, cv_heads, preferred_element_typ...  5.69 us
  transfers between devices with their start and end apart: 4, of which 2 were waited for; matrix products, arithmetic and copies ran while one was open for 8% of the time, Pallas kernels for 0%

commit v1 on v0

--- a/solution.py
+++ b/solution.py
@@ -1,8 +1,11 @@
+import functools
 import math
 
 import jax
 import jax.numpy as jnp
 from jax import lax
+from jax.experimental import pallas as pl
+from jax.experimental.pallas import tpu as pltpu
 from jax.sharding import PartitionSpec as P
 
 HEAD_SIZE = 64
@@ -201,9 +204,563 @@
     return (latent.astype(jnp.float32) + lat_gate * branch).astype(jnp.bfloat16)
 
 
+MESH = pl.DeviceIdType.MESH
+LANES = 128
+Q_ROWS = 80
+PIECES = 4
+F32 = jnp.float32
+BF16 = jnp.bfloat16
+
+
+def block_kernel(
+    sp_count,
+    latent_hbm,
+    cond_ref,
+    ctx_cond_ref,
+    context_hbm,
+    ms_hbm,
+    mc_hbm,
+    mg_hbm,
+    gain_ref,
+    wq_hbm,
+    wk_hbm,
+    wv_hbm,
+    wg_hbm,
+    wo_hbm,
+    sink_ref,
+    cos_ref,
+    sin_ref,
+    out_ref,
+    lat,
+    ctx_rows,
+    mods,
+    wq,
+    wk,
+    wv,
+    wg,
+    wo,
+    part,
+    part_in,
+    vecs,
+    modv,
+    hid,
+    ctx_hid,
+    qbuf,
+    gbuf,
+    kv,
+    ctx_kv,
+    mixed,
+    bsend,
+    brecv,
+    local_sem,
+    lat_sem,
+    part_sem,
+    vec_sem,
+    ctx_sem,
+    halo_sem,
+    out_sem,
+):
+    rank = lax.axis_index("sp")
+    side = lax.axis_index("tp")
+    other = 1 - side
+    own_rows, width = latent_hbm.shape
+    block = 2 * own_rows
+    mod_rows, mod_cols = ms_hbm.shape
+    kv_width = wk.shape[1]
+    q_width = wq.shape[1]
+    ctx_own = context_hbm.shape[0]
+    ctx_total = ctx_own * sp_count
+    kv_heads = kv_width // HEAD_SIZE
+    pairs = q_width // LANES // kv_heads
+    keys = Q_ROWS + 2 * WINDOW
+    span = -(-keys // LANES) * LANES
+    total_keys = span + ctx_total
+    piece = width // PIECES
+    chunks_own = own_rows // Q_ROWS
+    low_end = WINDOW + block
+
+    def load(src, dst, index):
+        return pltpu.make_async_copy(src, dst, local_sem.at[index])
+
+    own_at = pl.multiple_of(side * own_rows, 16)
+    far_at = pl.multiple_of(other * own_rows, 16)
+    loads = [
+        load(ms_hbm, mods.at[0], 0),
+        load(mc_hbm, mods.at[1], 1),
+        load(mg_hbm, mods.at[2], 2),
+        load(latent_hbm, lat.at[pl.ds(own_at, own_rows)], 3),
+        load(context_hbm, ctx_rows, 4),
+        load(wk_hbm, wk, 5),
+        load(wv_hbm, wv, 6),
+        load(wq_hbm, wq, 7),
+        load(wg_hbm, wg, 8),
+        load(wo_hbm, wo, 9),
+    ]
+    for copy in loads:
+        copy.start()
+
+    barrier = pltpu.get_barrier_semaphore()
+    pl.semaphore_signal(barrier, inc=1, device_id={"tp": other}, device_id_type=MESH)
+    for step in range(1, sp_count):
+        peer = lax.rem(rank + step, sp_count)
+        pl.semaphore_signal(barrier, inc=1, device_id={"sp": peer}, device_id_type=MESH)
+    pl.semaphore_wait(barrier, sp_count)
+
+    def lat_copy(c):
+        return pltpu.make_async_remote_copy(
+            src_ref=latent_hbm.at[pl.ds(c * Q_ROWS, Q_ROWS)],
+            dst_ref=lat.at[pl.ds(pl.multiple_of(own_at + c * Q_ROWS, 16), Q_ROWS)],
+            send_sem=lat_sem.at[0, c],
+            recv_sem=lat_sem.at[1, c],
+            device_id={"tp": other},
+            device_id_type=MESH,
+        )
+
+    lat_copies = [lat_copy(c) for c in range(chunks_own)]
+    lat_copies[0].start()
+
+    @pl.when(rank == 0)
+    def _():
+        kv[0:WINDOW, :] = jnp.zeros((WINDOW, 2 * kv_width), BF16)
+
+    @pl.when(rank == sp_count - 1)
+    def _():
+        kv[low_end : low_end + WINDOW, :] = jnp.zeros((WINDOW, 2 * kv_width), BF16)
+
+    first = pl.multiple_of(rank * mod_rows, LANES)
+    lat_c = cond_ref[:, pl.ds(first, mod_rows)]
+    ctx_c = ctx_cond_ref[:, pl.ds(first, mod_rows)]
+    row_id = lax.broadcasted_iota(jnp.int32, (16, mod_rows), 0)
+    both = jnp.where(row_id == 0, lat_c, ctx_c)
+    both = (both / (1.0 + jnp.exp(-both))).astype(BF16)
+    tile = mod_cols // 3
+    for m in range(3):
+        loads[m].wait()
+        for t in range(3):
+            cols = slice(t * tile, (t + 1) * tile)
+            prod = jnp.dot(both, mods[m, :, cols], preferred_element_type=F32)
+            part[2 * m : 2 * m + 2, cols] = prod[0:2, :]
+    part[6:8, :] = jnp.zeros((2, mod_cols), F32)
+
+    part_copies = []
+    for step in range(1, sp_count):
+        peer = lax.rem(rank + step, sp_count)
+        copy = pltpu.make_async_remote_copy(
+            src_ref=part,
+            dst_ref=part_in.at[step - 1],
+            send_sem=part_sem.at[0, step - 1],
+            recv_sem=part_sem.at[1, step - 1],
+            device_id={"sp": peer},
+            device_id_type=MESH,
+        )
+        copy.start()
+        part_copies.append(copy)
+    for copy in part_copies:
+        copy.wait()
+    summed = part[...]
+    for step in range(sp_count - 1):
+        summed = summed + part_in[step]
+    vecs[side] = summed
+    vec_copy = pltpu.make_async_remote_copy(
+        src_ref=vecs.at[side],
+        dst_ref=vecs.at[side],
+        send_sem=vec_sem.at[0],
+        recv_sem=vec_sem.at[1],
+        device_id={"tp": other},
+        device_id_type=MESH,
+    )
+    vec_copy.start()
+    for copy in lat_copies[1:]:
+        copy.start()
+    vec_copy.wait()
+    for h in range(2):
+        cols = slice(h * mod_cols, (h + 1) * mod_cols)
+        gain = gain_ref[:, cols]
+        modv[0:1, cols] = gain * (1.0 + vecs[h, 2:3, :])
+        modv[1:2, cols] = vecs[h, 0:1, :]
+        modv[2:3, cols] = gain * (1.0 + vecs[h, 3:4, :])
+        modv[3:4, cols] = vecs[h, 1:2, :]
+        modv[4:5, cols] = vecs[h, 4:5, :]
+
+    def modulate_rows(src, dst, begin, count, which):
+        def body(i, carry):
+            rows = pl.ds(pl.multiple_of(begin + i * 16, 16), 16)
+            values = src[rows, :].astype(F32)
+            mean = jnp.sum(values * values, axis=-1, keepdims=True) * (1.0 / width)
+            inverse = lax.rsqrt(mean + NORM_EPS)
+            scaled = values * inverse * modv[which : which + 1, :] + modv[which + 1 : which + 2, :]
+            dst[rows, :] = scaled.astype(BF16)
+            return carry
+
+        lax.fori_loop(0, count // 16, body, 0)
+
+    def turn(values, rows, factor):
+        lane = lax.broadcasted_iota(jnp.int32, values.shape, 1)
+        half = HEAD_SIZE // 2
+        ahead = pltpu.roll(values, LANES - half, 1)
+        behind = pltpu.roll(values, half, 1)
+        swapped = jnp.where(lane % HEAD_SIZE < half, ahead, behind)
+        turned = values * cos_ref[rows, :] + swapped * sin_ref[rows, :]
+        return turned * factor
+
+    def project_kv(begin):
+        rows = pl.ds(begin, own_rows)
+        into = pl.ds(pl.multiple_of(begin + WINDOW, 16), own_rows)
+        x = hid[rows, :]
+        k = jnp.dot(x, wk[...], preferred_element_type=F32)
+        for c in range(kv_width // LANES):
+            cols = slice(c * LANES, (c + 1) * LANES)
+            kv[into, cols] = turn(k[:, cols], rows, 1.0).astype(BF16)
+        v = jnp.dot(x, wv[...], preferred_element_type=F32)
+        kv[into, kv_width : 2 * kv_width] = v.astype(BF16)
+
+    step_cols = 2 * LANES
+
+    def project_q(begin):
+        rows = pl.ds(begin, own_rows)
+        factor = 1.0 / math.sqrt(HEAD_SIZE)
+
+        def body(t, carry):
+            at = pl.multiple_of(t * step_cols, step_cols)
+            y = jnp.dot(hid[rows, :], wq[:, pl.ds(at, step_cols)], preferred_element_type=F32)
+            for c in range(2):
+                cols = pl.ds(pl.multiple_of(at + c * LANES, LANES), LANES)
+                part_y = y[:, c * LANES : (c + 1) * LANES]
+                qbuf[rows, cols] = turn(part_y, rows, factor).astype(BF16)
+            return carry
+
+        lax.fori_loop(0, q_width // step_cols, body, 0)
+
+    def project_g(begin):
+        rows = pl.ds(begin, own_rows)
+
+        def body(t, carry):
+            cols = pl.ds(pl.multiple_of(t * step_cols, step_cols), step_cols)
+            y = jnp.dot(hid[rows, :], wg[:, cols], preferred_element_type=F32)
+            gbuf[rows, cols] = y.astype(BF16)
+            return carry
+
+        lax.fori_loop(0, q_width // step_cols, body, 0)
+
+    loads[4].wait()
+    modulate_rows(ctx_rows, ctx_hid, 0, ctx_own, 2)
+    loads[5].wait()
+    loads[6].wait()
+    ctx_at = pl.ds(pl.multiple_of(rank * ctx_own, 16), ctx_own)
+    xc = ctx_hid[...]
+    ctx_kv[ctx_at, 0:kv_width] = jnp.dot(xc, wk[...], preferred_element_type=F32).astype(BF16)
+    ctx_kv[ctx_at, kv_width : 2 * kv_width] = jnp.dot(
+        xc, wv[...], preferred_element_type=F32
+    ).astype(BF16)
+    ctx_copies = []
+    for step in range(1, sp_count):
+        peer = lax.rem(rank + step, sp_count)
+        copy = pltpu.make_async_remote_copy(
+            src_ref=ctx_kv.at[ctx_at],
+            dst_ref=ctx_kv.at[ctx_at],
+            send_sem=ctx_sem.at[0, step - 1],
+            recv_sem=ctx_sem.at[1, step - 1],
+            device_id={"sp": peer},
+            device_id_type=MESH,
+        )
+        copy.start()
+        ctx_copies.append(copy)
+
+    def halo(src_at, dst_at, index, target):
+        return pltpu.make_async_remote_copy(
+            src_ref=kv.at[pl.ds(pl.multiple_of(src_at, 16), WINDOW)],
+            dst_ref=kv.at[pl.ds(pl.multiple_of(dst_at, 16), WINDOW)],
+            send_sem=halo_sem.at[0, index],
+            recv_sem=halo_sem.at[1, index],
+            device_id={"sp": target},
+            device_id_type=MESH,
+        )
+
+    early_to = rank - 1 + 2 * side
+    late_to = rank + 1 - 2 * side
+    has_early_to = (early_to >= 0) & (early_to < sp_count)
+    has_late_to = (late_to >= 0) & (late_to < sp_count)
+    early = halo(WINDOW + side * (block - WINDOW), other * low_end, 0, early_to)
+    late = halo(WINDOW + other * (block - WINDOW), side * low_end, 1, late_to)
+
+    loads[3].wait()
+    modulate_rows(lat, hid, own_at, own_rows, 0)
+    project_kv(own_at)
+
+    @pl.when(has_early_to)
+    def _():
+        early.start()
+
+    loads[7].wait()
+    project_q(own_at)
+    loads[8].wait()
+    project_g(own_at)
+
+    for c in range(chunks_own):
+        lat_copies[c].wait()
+        modulate_rows(lat, hid, pl.multiple_of(far_at + c * Q_ROWS, 16), Q_ROWS, 0)
+    project_kv(far_at)
+
+    @pl.when(has_late_to)
+    def _():
+        late.start()
+
+    project_q(far_at)
+    project_g(far_at)
+    for copy in ctx_copies:
+        copy.wait()
+
+    @pl.when(has_late_to)
+    def _():
+        early.wait_recv()
+
+    loads[9].wait()
+
+    def attend_rows(begin):
+        rows = pl.ds(begin, Q_ROWS)
+        i = lax.broadcasted_iota(jnp.int32, (Q_ROWS, span), 0)
+        j = lax.broadcasted_iota(jnp.int32, (Q_ROWS, span), 1)
+        offset = j - i
+        k_pos = rank * block + begin - WINDOW + j
+        allowed = (offset >= 0) & (offset <= 2 * WINDOW) & (k_pos >= 0)
+        allowed = allowed & (k_pos < block * sp_count)
+        bias = jnp.where(allowed, 0.0, MASK_VALUE)
+        lane = lax.broadcasted_iota(jnp.int32, (total_keys, LANES), 1)
+        low_lane = lane < HEAD_SIZE
+        filler = jnp.zeros((span - keys, LANES), BF16)
+        out_low = lax.broadcasted_iota(jnp.int32, (Q_ROWS, LANES), 1) < HEAD_SIZE
+
+        def both_heads(at):
+            cols = slice(at, at + LANES)
+            tile_kv = jnp.concatenate(
+                [kv[pl.ds(begin, keys), cols], filler, ctx_kv[:, cols]], axis=0
+            ).astype(F32)
+            turned = pltpu.roll(tile_kv, HEAD_SIZE, 1)
+            even = jnp.concatenate(
+                [jnp.where(low_lane, tile_kv, 0.0), jnp.where(low_lane, 0.0, turned)], axis=0
+            )
+            odd = jnp.concatenate(
+                [jnp.where(low_lane, turned, 0.0), jnp.where(low_lane, 0.0, tile_kv)], axis=0
+            )
+            return even.astype(BF16), odd.astype(BF16)
+
+        for tile_id in range(kv_heads // 2):
+            k_two = both_heads(tile_id * LANES)
+            v_two = both_heads(kv_width + tile_id * LANES)
+            for parity in range(2):
+                head = 2 * tile_id + parity
+                k_wide = k_two[parity]
+                v_wide = v_two[parity]
+                base = head * pairs
+                for p in range(pairs):
+                    cols = slice((base + p) * LANES, (base + p + 1) * LANES)
+                    scores = lax.dot_general(
+                        qbuf[rows, cols],
+                        k_wide,
+                        (((1,), (1,)), ((), ())),
+                        preferred_element_type=F32,
+                    )
+                    exps = []
+                    scale = []
+                    for h in range(2):
+                        sink = sink_ref[2 * (base + p) + h]
+                        near = scores[:, h * total_keys : h * total_keys + span] + bias
+                        far = scores[:, h * total_keys + span : (h + 1) * total_keys]
+                        peak = jnp.maximum(
+                            jnp.max(near, axis=-1, keepdims=True),
+                            jnp.max(far, axis=-1, keepdims=True),
+                        )
+                        peak = jnp.maximum(peak, sink)
+                        near = jnp.exp(near - peak)
+                        far = jnp.exp(far - peak)
+                        total = (
+                            jnp.sum(near, axis=-1, keepdims=True)
+                            + jnp.sum(far, axis=-1, keepdims=True)
+                            + jnp.exp(sink - peak)
+                        )
+                        exps += [near.astype(BF16), far.astype(BF16)]
+                        scale.append(1.0 / total)
+                    weights = jnp.concatenate(exps, axis=1)
+                    result = jnp.dot(weights, v_wide, preferred_element_type=F32)
+                    result = result * jnp.where(out_low, scale[0], scale[1])
+                    gate = gbuf[rows, cols].astype(F32)
+                    gate = gate / (1.0 + jnp.exp(-gate))
+                    mixed[:, cols] = (result * gate).astype(BF16)
+
+    def out_copy(c, n):
+        return pltpu.make_async_remote_copy(
+            src_ref=bsend.at[c, n],
+            dst_ref=brecv.at[c, n],
+            send_sem=out_sem.at[0, c, n],
+            recv_sem=out_sem.at[1, c, n],
+            device_id={"tp": other},
+            device_id_type=MESH,
+        )
+
+    def far_chunk(c, carry):
+        attend_rows(pl.multiple_of(far_at + c * Q_ROWS, 16))
+
+        def product(n, inner):
+            cols = pl.ds(pl.multiple_of(n * piece, LANES), piece)
+            y = jnp.dot(mixed[...], wo[:, cols], preferred_element_type=F32)
+            bsend[c, n] = y.astype(BF16)
+            out_copy(c, n).start()
+            return inner
+
+        lax.fori_loop(0, PIECES, product, 0)
+        return carry
+
+    lax.fori_loop(0, chunks_own, far_chunk, 0)
+
+    @pl.when(has_early_to)
+    def _():
+        early.wait_send()
+        late.wait_recv()
+
+    @pl.when(has_late_to)
+    def _():
+        late.wait_send()
+
+    def own_chunk(c, carry):
+        attend_rows(pl.multiple_of(own_at + c * Q_ROWS, 16))
+
+        def product(n, inner):
+            cols = pl.ds(pl.multiple_of(n * piece, LANES), piece)
+            y = jnp.dot(mixed[...], wo[:, cols], preferred_element_type=F32)
+            out_ref[pl.ds(pl.multiple_of(c * Q_ROWS, 16), Q_ROWS), cols] = y.astype(BF16)
+            return inner
+
+        lax.fori_loop(0, PIECES, product, 0)
+        return carry
+
+    lax.fori_loop(0, chunks_own, own_chunk, 0)
+
+    def finish(s, carry):
+        c = s // PIECES
+        n = s % PIECES
+        out_copy(c, n).wait()
+        cols = pl.ds(pl.multiple_of(n * piece, LANES), piece)
+        rows = pl.ds(pl.multiple_of(c * Q_ROWS, 16), Q_ROWS)
+        lat_at = pl.ds(pl.multiple_of(own_at + c * Q_ROWS, 16), Q_ROWS)
+        branch = out_ref[rows, cols].astype(F32) + brecv[c, n].astype(F32)
+        moved = lat[lat_at, cols].astype(F32) + modv[4:5, cols] * branch
+        out_ref[rows, cols] = moved.astype(BF16)
+        return carry
+
+    lax.fori_loop(0, chunks_own * PIECES, finish, 0)
+
+
+def rotation_tables(sp_rank, block_rows):
+    positions = sp_rank * block_rows + jnp.arange(block_rows, dtype=jnp.int32)
+    quarter = HEAD_SIZE // 4
+    inverse = jnp.exp(-math.log(10000.0) * jnp.arange(quarter, dtype=jnp.float32) / quarter)
+    grid_row = (positions // GRID_W).astype(jnp.float32)
+    mesh_column = (positions % GRID_W).astype(jnp.float32)
+    angles = jnp.concatenate([grid_row[:, None] * inverse, mesh_column[:, None] * inverse], axis=1)
+    cosine = jnp.cos(angles)
+    sine = jnp.sin(angles)
+    copies = LANES // HEAD_SIZE
+    return (
+        jnp.concatenate([cosine, cosine] * copies, axis=1),
+        jnp.concatenate([-sine, sine] * copies, axis=1),
+    )
+
+
+def fused_shards(
+    latent,
+    condition,
+    ctx_condition,
+    context,
+    mod_shift,
+    mod_scale,
+    mod_gate,
+    norm_gain,
+    w_query,
+    key_weight,
+    value_weight,
+    w_gate,
+    w_out,
+    sink_logit,
+):
+    sp_count = lax.axis_size("sp")
+    rows, width = latent.shape
+    block = 2 * rows
+    mod_rows, mod_cols = mod_shift.shape
+    q_width = w_query.shape[1]
+    kv_width = key_weight.shape[1]
+    ctx_own = context.shape[0]
+    cosine, sine = rotation_tables(lax.axis_index("sp"), block)
+    kv_rows = block + 2 * WINDOW
+    chunks = rows // Q_ROWS
+    piece = width // PIECES
+    anywhere = pl.BlockSpec(memory_space=pl.ANY)
+    vmem = pl.BlockSpec(memory_space=pltpu.VMEM)
+    smem = pl.BlockSpec(memory_space=pltpu.SMEM)
+    dma = pltpu.SemaphoreType.DMA
+    return pl.pallas_call(
+        functools.partial(block_kernel, sp_count),
+        out_shape=jax.ShapeDtypeStruct((rows, width), BF16),
+        in_specs=[anywhere, vmem, vmem, anywhere, anywhere, anywhere, anywhere, vmem]
+        + [anywhere] * 5
+        + [smem, vmem, vmem],
+        out_specs=vmem,
+        scratch_shapes=[
+            pltpu.VMEM((block, width), BF16),
+            pltpu.VMEM((ctx_own, width), BF16),
+            pltpu.VMEM((3, mod_rows, mod_cols), BF16),
+            pltpu.VMEM((width, q_width), BF16),
+            pltpu.VMEM((width, kv_width), BF16),
+            pltpu.VMEM((width, kv_width), BF16),
+            pltpu.VMEM((width, q_width), BF16),
+            pltpu.VMEM((q_width, width), BF16),
+            pltpu.VMEM((8, mod_cols), F32),
+            pltpu.VMEM((sp_count - 1, 8, mod_cols), F32),
+            pltpu.VMEM((2, 8, mod_cols), F32),
+            pltpu.VMEM((8, width), F32),
+            pltpu.VMEM((block, width), BF16),
+            pltpu.VMEM((ctx_own, width), BF16),
+            pltpu.VMEM((block, q_width), BF16),
+            pltpu.VMEM((block, q_width), BF16),
+            pltpu.VMEM((kv_rows, 2 * kv_width), BF16),
+            pltpu.VMEM((ctx_own * sp_count, 2 * kv_width), BF16),
+            pltpu.VMEM((Q_ROWS, q_width), BF16),
+            pltpu.VMEM((chunks, PIECES, Q_ROWS, piece), BF16),
+            pltpu.VMEM((chunks, PIECES, Q_ROWS, piece), BF16),
+            dma((10,)),
+            dma((2, chunks)),
+            dma((2, sp_count - 1)),
+            dma((2,)),
+            dma((2, sp_count - 1)),
+            dma((2, 2)),
+            dma((2, chunks, PIECES)),
+        ],
+        compiler_params=pltpu.CompilerParams(
+            collective_id=0, has_side_effects=True, vmem_limit_bytes=62 * 1024 * 1024
+        ),
+        name="block_kernel",
+    )(
+        latent,
+        condition[None, :],
+        ctx_condition[None, :],
+        context,
+        mod_shift,
+        mod_scale,
+        mod_gate,
+        norm_gain[None, :],
+        w_query,
+        key_weight,
+        value_weight,
+        w_gate,
+        w_out,
+        sink_logit,
+        cosine,
+        sine,
+    )
+
+
 def solution(mesh):
     return jax.shard_map(
-        shards,
+        fused_shards if mesh.shape["tp"] == 2 else shards,
         mesh=mesh,
         in_specs=(
             P(("dp", "sp", "tp"), None),

time: 180 us -> 69.9 us (0.39)
  Pallas kernels: 0 us -> 65.2 us
  matrix products: 55 us -> 0 us
  waiting for transfers between devices: 44.9 us -> 0 us
  blocking collectives: 39.5 us -> 0 us
  between operations: 13.7 us -> 0.04 us
  other arithmetic: 14.8 us -> 2.03 us
  starting transfers between devices: 4.91 us -> 0 us
  local copies, waits for them, and re-layouts: 6.34 us -> 2.42 us
    pallas_call x0 -> x1, Pallas kernels: none -> 65.2 us  [fused_shards(): pl.pallas_call(functools.partial(block_kernel, sp_count), out_shape=jax.S...]
    dot_general x13 -> x0, matrix products: 55 us -> none  [the longest x1 14.5 us: shards(): jnp.dot(mixed, w_out, preferred_element_type=jnp.float32)]
    reduce_scatter x1 -> x0, waiting for transfers between devices: 31.8 us -> none  [shards(): lax.psum_scatter(jnp.dot(mixed, w_out, preferred_element_type=jnp.float32...]
    psum x1 -> x0, blocking collectives: 21.4 us -> none  [shards(): summed = lax.psum(partial_value, 'sp')]
    all_gather x2 -> x0, blocking collectives: 18.1 us -> none  [the longest x1 13.4 us: shards(): ctx_all = lax.all_gather(ctx_pair, 'sp', axis=0, tiled=True)]
    all_gather x1 -> x0, waiting for transfers between devices: 13.1 us -> none  [shards(): row_piece = lax.all_gather(hidden, 'tp', axis=0, tiled=True)]
    reduce_sum x4 -> x0, other arithmetic: 8.45 us -> none  [the longest x1 5.45 us: attend(): jnp.sum(near_exp, axis=-1, keepdims=True)]
    ppermute x2 -> x0, starting transfers between devices: 4.87 us -> none  [the longest x1 3.39 us: with_halo(): lax.ppermute(lax.slice_in_dim(block, block.shape[dim] - width, None, axis...]
  transfers between devices with their start and end apart: 4 -> 0, of which waited for: 2 -> 0; matrix products, arithmetic and copies ran while one was open for 8% -> 0% of each run, Pallas kernels for 0% -> 0%
where the time goes in v1:
time: 69.9 us; the launch traced here: 69.7 us
  Pallas kernels  65.2 us (93%)
  local copies, waits for them, and re-layouts  2.42 us (3%)
  other arithmetic  2.03 us (3%)
    pallas_call x1, Pallas kernels, fused_shards(): pl.pallas_call(functools.partial(block_kernel, sp_count), out_shape=jax.S...  65.2 us
    unnamed x1, local copies, waits for them, and re-layouts  2.21 us

profile of v1, /device:TPU:0, one launch (start us, length us, event | category | flops | bytes accessed | tf_op | source)
XLA Modules:
  0.0 69.7 jit_solution(8600088946657328542)
XLA Ops:
  0.0 0.1 broadcast_multiply_fusion.1
  0.1 0.2 fusion
  0.3 0.1 copy.21
  0.4 0.9 %pad_maximum_fusion.1.sin_ref = f32[320,128]{1,0:T(8,128)} fusion(f32[320,32]{1,0:T(8,128)S(1)} %copy.21, f32[320,32]{1,0:T(8,128)S(1)} %neg.3), kind=kLoop, calls=%fused_computation.1 | loop fusion | flops 122880 | bytes 245760 | tf_op jit(solution)/shard_map/concatenate | solution.py:665
  1.3 0.1 copy.17
  1.4 0.9 %pad_maximum_fusion.cos_ref = f32[320,128]{1,0:T(8,128)} fusion(f32[320,32]{1,0:T(8,128)S(1)} %copy.17), kind=kLoop, calls=%fused_computation | loop fusion | flops 122880 | bytes 204800 | tf_op jit(solution)/shard_map/concatenate | solution.py:664
  2.3 65.2 %block_kernel.1 = bf16[160,3072]{1,0:T(8,128)(2,1)} custom-call(bf16[160,3072]{1,0:T(8,128)(2,1)} %latent_hbm.1, f32[1,3072]{1,0:T(1,128)} %bitcast.3, f32[1,3072]{1,0:T(1,128)} %bitcast.4, bf16[32,3072]{1,0:T(8,128)(2,1)} %context_hbm.1, bf16[768,1536]{1,0:T(8,128)(2,1)} %ms_hbm.1, bf16[768,1536]{1,0:T(8,128)(2,1)} %mc_hbm.1, bf16[768,1536]{1,0:T(8,128)(2,1)} %mg_hbm.1, ...), custom_call_target="tpu_custom_call" | custom-call | tf_op jit(solution)/shard_map/block_kernel/pallas_call | solution.py:700
  67.5 2.2 %copy.25 = bf16[160,3072]{1,0:T(8,128)(2,1)} copy(bf16[160,3072]{1,0:T(8,128)(2,1)} %block_kernel.1) | data formatting | bytes 1966080
  (3 shorter events, 0.0 us)

commit v2 on v1

--- a/solution.py
+++ b/solution.py
@@ -228,9 +228,10 @@
     wg_hbm,
     wo_hbm,
     sink_ref,
+    out_hbm,
+    out_ref,
     cos_ref,
     sin_ref,
-    out_ref,
     lat,
     ctx_rows,
     mods,
@@ -259,6 +260,7 @@
     ctx_sem,
     halo_sem,
     out_sem,
+    store_sem,
 ):
     rank = lax.axis_index("sp")
     side = lax.axis_index("tp")
@@ -296,7 +298,7 @@
         load(wg_hbm, wg, 8),
         load(wo_hbm, wo, 9),
     ]
-    for copy in loads:
+    for copy in loads[0:5]:
         copy.start()
 
     barrier = pltpu.get_barrier_semaphore()
@@ -340,6 +342,8 @@
             cols = slice(t * tile, (t + 1) * tile)
             prod = jnp.dot(both, mods[m, :, cols], preferred_element_type=F32)
             part[2 * m : 2 * m + 2, cols] = prod[0:2, :]
+    for copy in loads[5:]:
+        copy.start()
     part[6:8, :] = jnp.zeros((2, mod_cols), F32)
 
     part_copies = []
@@ -355,6 +359,22 @@
         )
         copy.start()
         part_copies.append(copy)
+
+    def table_rows(g, carry):
+        rows = pl.ds(pl.multiple_of(g * 32, 32), 32)
+        lane = lax.broadcasted_iota(jnp.int32, (32, LANES), 1)
+        position = rank * block + g * 32 + lax.broadcasted_iota(jnp.int32, (32, LANES), 0)
+        quarter = HEAD_SIZE // 4
+        inverse = jnp.exp(-math.log(10000.0) * (lane % quarter).astype(F32) / quarter)
+        in_row = lane % (2 * quarter) < quarter
+        place = jnp.where(in_row, position // GRID_W, position % GRID_W).astype(F32)
+        angles = place * inverse
+        cos_ref[rows, :] = jnp.cos(angles)
+        sine = jnp.sin(angles)
+        sin_ref[rows, :] = jnp.where(lane % HEAD_SIZE < 2 * quarter, -sine, sine)
+        return carry
+
+    lax.fori_loop(0, block // 32, table_rows, 0)
     for copy in part_copies:
         copy.wait()
     summed = part[...]
@@ -403,9 +423,9 @@
         turned = values * cos_ref[rows, :] + swapped * sin_ref[rows, :]
         return turned * factor
 
-    def project_kv(begin):
-        rows = pl.ds(begin, own_rows)
-        into = pl.ds(pl.multiple_of(begin + WINDOW, 16), own_rows)
+    def project_kv(begin, count):
+        rows = pl.ds(begin, count)
+        into = pl.ds(pl.multiple_of(begin + WINDOW, 16), count)
         x = hid[rows, :]
         k = jnp.dot(x, wk[...], preferred_element_type=F32)
         for c in range(kv_width // LANES):
@@ -416,8 +436,8 @@
 
     step_cols = 2 * LANES
 
-    def project_q(begin):
-        rows = pl.ds(begin, own_rows)
+    def project_q(begin, count):
+        rows = pl.ds(begin, count)
         factor = 1.0 / math.sqrt(HEAD_SIZE)
 
         def body(t, carry):
@@ -431,8 +451,8 @@
 
         lax.fori_loop(0, q_width // step_cols, body, 0)
 
-    def project_g(begin):
-        rows = pl.ds(begin, own_rows)
+    def project_g(begin, count):
+        rows = pl.ds(begin, count)
 
         def body(t, carry):
             cols = pl.ds(pl.multiple_of(t * step_cols, step_cols), step_cols)
@@ -485,28 +505,27 @@
 
     loads[3].wait()
     modulate_rows(lat, hid, own_at, own_rows, 0)
-    project_kv(own_at)
+    project_kv(own_at, own_rows)
 
     @pl.when(has_early_to)
     def _():
         early.start()
 
-    loads[7].wait()
-    project_q(own_at)
-    loads[8].wait()
-    project_g(own_at)
-
     for c in range(chunks_own):
+        chunk_at = pl.multiple_of(far_at + c * Q_ROWS, 16)
         lat_copies[c].wait()
-        modulate_rows(lat, hid, pl.multiple_of(far_at + c * Q_ROWS, 16), Q_ROWS, 0)
-    project_kv(far_at)
+        modulate_rows(lat, hid, chunk_at, Q_ROWS, 0)
+        project_kv(chunk_at, Q_ROWS)
+        if c == 0:
+            loads[7].wait()
+            project_q(chunk_at, Q_ROWS)
+            loads[8].wait()
+            project_g(chunk_at, Q_ROWS)
 
     @pl.when(has_late_to)
     def _():
         late.start()
 
-    project_q(far_at)
-    project_g(far_at)
     for copy in ctx_copies:
         copy.wait()
 
@@ -598,7 +617,14 @@
         )
 
     def far_chunk(c, carry):
-        attend_rows(pl.multiple_of(far_at + c * Q_ROWS, 16))
+        chunk_at = pl.multiple_of(far_at + c * Q_ROWS, 16)
+
+        @pl.when(c > 0)
+        def _():
+            project_q(chunk_at, Q_ROWS)
+            project_g(chunk_at, Q_ROWS)
+
+        attend_rows(chunk_at)
 
         def product(n, inner):
             cols = pl.ds(pl.multiple_of(n * piece, LANES), piece)
@@ -611,6 +637,8 @@
         return carry
 
     lax.fori_loop(0, chunks_own, far_chunk, 0)
+    project_q(own_at, own_rows)
+    project_g(own_at, own_rows)
 
     @pl.when(has_early_to)
     def _():
@@ -634,6 +662,13 @@
         return carry
 
     lax.fori_loop(0, chunks_own, own_chunk, 0)
+
+    def store(c, n):
+        cols = pl.ds(pl.multiple_of(n * piece, LANES), piece)
+        rows = pl.ds(pl.multiple_of(c * Q_ROWS, 16), Q_ROWS)
+        return pltpu.make_async_copy(
+            out_ref.at[rows, cols], out_hbm.at[rows, cols], store_sem.at[c, n]
+        )
 
     def finish(s, carry):
         c = s // PIECES
@@ -645,25 +680,13 @@
         branch = out_ref[rows, cols].astype(F32) + brecv[c, n].astype(F32)
         moved = lat[lat_at, cols].astype(F32) + modv[4:5, cols] * branch
         out_ref[rows, cols] = moved.astype(BF16)
+        store(c, n).start()
         return carry
 
     lax.fori_loop(0, chunks_own * PIECES, finish, 0)
-
-
-def rotation_tables(sp_rank, block_rows):
-    positions = sp_rank * block_rows + jnp.arange(block_rows, dtype=jnp.int32)
-    quarter = HEAD_SIZE // 4
-    inverse = jnp.exp(-math.log(10000.0) * jnp.arange(quarter, dtype=jnp.float32) / quarter)
-    grid_row = (positions // GRID_W).astype(jnp.float32)
-    mesh_column = (positions % GRID_W).astype(jnp.float32)
-    angles = jnp.concatenate([grid_row[:, None] * inverse, mesh_column[:, None] * inverse], axis=1)
-    cosine = jnp.cos(angles)
-    sine = jnp.sin(angles)
-    copies = LANES // HEAD_SIZE
-    return (
-        jnp.concatenate([cosine, cosine] * copies, axis=1),
-        jnp.concatenate([-sine, sine] * copies, axis=1),
-    )
+    for c in range(chunks_own):
+        for n in range(PIECES):
+            store(c, n).wait()
 
 
 def fused_shards(
@@ -689,7 +712,6 @@
     q_width = w_query.shape[1]
     kv_width = key_weight.shape[1]
     ctx_own = context.shape[0]
-    cosine, sine = rotation_tables(lax.axis_index("sp"), block)
     kv_rows = block + 2 * WINDOW
     chunks = rows // Q_ROWS
     piece = width // PIECES
@@ -702,9 +724,12 @@
         out_shape=jax.ShapeDtypeStruct((rows, width), BF16),
         in_specs=[anywhere, vmem, vmem, anywhere, anywhere, anywhere, anywhere, vmem]
         + [anywhere] * 5
-        + [smem, vmem, vmem],
-        out_specs=vmem,
+        + [smem],
+        out_specs=anywhere,
         scratch_shapes=[
+            pltpu.VMEM((rows, width), BF16),
+            pltpu.VMEM((block, LANES), F32),
+            pltpu.VMEM((block, LANES), F32),
             pltpu.VMEM((block, width), BF16),
             pltpu.VMEM((ctx_own, width), BF16),
             pltpu.VMEM((3, mod_rows, mod_cols), BF16),
@@ -733,6 +758,7 @@
             dma((2, sp_count - 1)),
             dma((2, 2)),
             dma((2, chunks, PIECES)),
+            dma((chunks, PIECES)),
         ],
         compiler_params=pltpu.CompilerParams(
             collective_id=0, has_side_effects=True, vmem_limit_bytes=62 * 1024 * 1024
@@ -753,8 +779,6 @@
         w_gate,
         w_out,
         sink_logit,
-        cosine,
-        sine,
     )
 
 

time: 69.9 us -> 72.6 us (1.039)
  Pallas kernels: 65.2 us -> 70.2 us
  other arithmetic: 2.03 us -> 0 us
    pallas_call x1, Pallas kernels: 65.2 us -> 70.2 us  [fused_shards(): pl.pallas_call(functools.partial(block_kernel, sp_count), out_shape=jax.S...]
    concatenate x2 -> x0, other arithmetic: 1.74 us -> none  [the longest x1 0.87 us: rotation_tables(): jnp.concatenate([cosine, cosine] * copies, axis=1)]
where the time goes in v2:
time: 72.6 us; the launch traced here: 72.4 us
  Pallas kernels  70.2 us (97%)
  local copies, waits for them, and re-layouts  2.21 us (3%)
    pallas_call x1, Pallas kernels, fused_shards(): pl.pallas_call(functools.partial(block_kernel, sp_count), out_shape=jax.S...  70.2 us
    unnamed x1, local copies, waits for them, and re-layouts  2.21 us

profile of v2, /device:TPU:0, one launch (start us, length us, event | category | flops | bytes accessed | tf_op | source)
XLA Modules:
  0.0 72.4 jit_solution(13394724165959720116)
XLA Ops:
  0.0 70.2 %block_kernel.1 = bf16[160,3072]{1,0:T(8,128)(2,1)} custom-call(bf16[160,3072]{1,0:T(8,128)(2,1)} %latent_hbm.1, f32[1,3072]{1,0:T(1,128)} %bitcast.3, f32[1,3072]{1,0:T(1,128)} %bitcast.4, bf16[32,3072]{1,0:T(8,128)(2,1)} %context_hbm.1, bf16[768,1536]{1,0:T(8,128)(2,1)} %ms_hbm.1, bf16[768,1536]{1,0:T(8,128)(2,1)} %mc_hbm.1, bf16[768,1536]{1,0:T(8,128)(2,1)} %mg_hbm.1, ...), custom_call_target="tpu_custom_call" | custom-call | tf_op jit(solution)/shard_map/block_kernel/pallas_call | solution.py:722
  70.2 2.2 %copy.16 = bf16[160,3072]{1,0:T(8,128)(2,1)} copy(bf16[160,3072]{1,0:T(8,128)(2,1)} %block_kernel.1) | data formatting | bytes 1966080
